TPU v7x, 32 devices: a whole 2x2x4 slice. The times are simulated.
32 devices in a mesh: ep: 4 (over y, x), tp: 8 (over z, core).
Axes of the slice: x: 2, y: 2, z: 4, core: 2. Of those that a mesh axis runs over, the one named last changes fastest.
Arguments:
- tokens: bfloat16 [1024, 2048], P('ep', 'tp'), may hold values from -600 to 600
- pre_gain: float32 [2048], P('tp'), may hold values from 0.1 to 1.9
- expert_gate: bfloat16 [4, 2048, 8192], P('ep', None, 'tp'), may hold values from -0.125 to 0.125
- expert_up: bfloat16 [4, 2048, 8192], P('ep', None, 'tp'), may hold values from -0.125 to 0.125
- expert_down: bfloat16 [4, 8192, 2048], P('ep', 'tp'), may hold values from -8 to 8
- routes: int32 [1024, 2], P('ep'), may hold values from 0 to 3, all different within a row; in each aligned block of 256 rows (0 to 255, 256 to 511, ...) at most 192 rows name the same one
- route_weights: float32 [1024, 2], P('ep'), may hold values from 0.1 to 1
- post_gain: float32 [2048], P('tp'), may hold values from 0.1 to 1.9
Outputs:
- layer_out: bfloat16 [1024, 2048], P('ep', 'tp')
Inputs may be any that keep to these rules, and one draw needn't show every extreme that they name: `routes`: each token names 2 different experts. Among the 256 tokens of one index of ep no expert is named more than 192 times, a bound that some expert reaches in some of these blocks.
All inputs are finite; a program needn't handle non-finite values.
Results may differ from a plain program's by a relative error of at most 0.024.
Values may be sent and summed in bfloat16 or wider, within the bound.
A program may use at most 64 MiB of HBM per device.

v0:
```python
import jax
import jax.numpy as jnp
from jax import lax
from jax.sharding import PartitionSpec as P

EPSILON = 1e-06


def local(tokens, pre_gain, expert_gate, expert_up, expert_down, routes, route_weights, post_gain):
    local_experts = expert_gate.shape[0]
    groups = lax.axis_size("ep")
    experts_all = local_experts * groups
    tok_rows, part_width = tokens.shape
    full_width = part_width * lax.axis_size("tp")
    capacity = 3 * tok_rows // experts_all
    values = tokens.astype(jnp.float32)
    input_sq = lax.psum(jnp.sum(values * values, axis=-1), "tp")
    normed = (
        values * lax.rsqrt(input_sq / full_width + EPSILON)[:, None] * pre_gain[None, :]
    ).astype(jnp.bfloat16)
    onehot = (routes[:, :, None] == jnp.arange(experts_all, dtype=jnp.int32)).astype(jnp.int32)
    onehot = onehot.reshape(tok_rows * 2, experts_all)
    earlier = jnp.cumsum(onehot, axis=0) - onehot
    slots = jnp.sum(earlier * onehot, axis=-1).reshape(tok_rows, 2)
    positions = routes * capacity + slots
    places = jnp.arange(experts_all * capacity, dtype=jnp.int32)
    first_pick = (places[:, None] == positions[None, :, 0]).astype(jnp.bfloat16)
    second_pick = (places[:, None] == positions[None, :, 1]).astype(jnp.bfloat16)
    dispatch = first_pick + second_pick
    outgoing = jnp.dot(dispatch, normed, preferred_element_type=jnp.float32).astype(jnp.bfloat16)
    arrived = lax.all_to_all(outgoing, "ep", split_axis=0, concat_axis=0, tiled=True)
    fragment = lax.all_gather(arrived, "tp", axis=1, tiled=True)
    count = fragment.shape[1]
    grouped = fragment.reshape(groups, local_experts, capacity, count)
    gate_pre = jnp.einsum(
        "secw,ewf->secf", grouped, expert_gate, preferred_element_type=jnp.float32
    )
    up_pre = jnp.einsum("secw,ewf->secf", grouped, expert_up, preferred_element_type=jnp.float32)
    hidden = (jax.nn.silu(gate_pre) * up_pre).astype(jnp.bfloat16)
    product = jnp.einsum("secf,efd->dsec", hidden, expert_down, preferred_element_type=jnp.float32)
    summed = lax.psum_scatter(
        product.reshape(lax.axis_size("tp") * part_width, groups * local_experts * capacity).astype(
            jnp.bfloat16
        ),
        "tp",
        scatter_dimension=0,
        tiled=True,
    )
    returned = lax.all_to_all(summed, "ep", split_axis=1, concat_axis=1, tiled=True)
    contract = (((0,), (1,)), ((), ()))
    first_out = lax.dot_general(first_pick, returned, contract, preferred_element_type=jnp.float32)
    second_out = lax.dot_general(
        second_pick, returned, contract, preferred_element_type=jnp.float32
    )
    combined = route_weights[:, 0:1] * first_out + route_weights[:, 1:2] * second_out
    output_sq = lax.psum(jnp.sum(combined * combined, axis=-1), "tp")
    scaled = combined * lax.rsqrt(output_sq / full_width + EPSILON)[:, None] * post_gain[None, :]
    return scaled.astype(jnp.bfloat16)


def solution(mesh):
    placed = (
        P("ep", "tp"),
        P("tp"),
        P("ep", None, "tp"),
        P("ep", None, "tp"),
        P("ep", "tp", None),
        P("ep", None),
        P("ep", None),
        P("tp"),
    )
    return jax.shard_map(
        local, mesh=mesh, in_specs=placed, out_specs=P("ep", "tp"), check_vma=False
    )
```

profile of v0, /device:TPU:0, one launch (start us, length us, event | category | flops | bytes accessed | tf_op | source)
XLA Modules:
  0.0 164.0 jit_solution(8557718616161930768)
XLA Ops:
  6.5 0.0 all-gather.2.cloned.1.call-start
  6.5 0.8 copy.20
  7.4 0.1 eq.61
  7.5 0.1 eq.57
  7.7 1.2 reduce-window.6
  8.9 0.2 slice_reduce_fusion
  9.1 0.2 reduce-window.9
  9.3 0.1 add_bitcast_fusion
  9.4 0.1 reshape.55
  9.5 0.1 copy.22
  9.6 0.7 multiply_add_fusion
  10.3 1.0 fusion.28
  11.3 18.1 %psum.14 = f32[256]{0:T(256)S(1)} all-reduce(f32[256]{0:T(256)S(1)} %fusion.28), channel_id=1, replica_groups=mesh['ep'=4,'tp'=8] {'tp'}, use_global_device_ids=true, to_apply=%region_4.5 | all-reduce | flops 256 | bytes 2048 | tf_op jit(solution)/shard_map/psum | solution.py:17
  29.4 1.3 convolution_convert_fusion
  30.7 10.1 %all_to_all.24 = bf16[4,192,256]{2,1,0:T(8,128)(2,1)} all-to-all(bf16[4,192,256]{2,1,0:T(8,128)(2,1)S(1)} %bitcast.82), channel_id=1, replica_groups=mesh['ep'=4,'tp'=8] {'ep'}, dimensions={0} | all-to-all | bytes 786432 | tf_op jit(solution)/shard_map/all_to_all | solution.py:31
  40.8 0.0 all-gather.2.cloned.1.call-update
  40.8 0.0 reduce-scatter.2.cloned.1.call-start
  40.8 35.9 %all-gather.2.cloned.1.call-done = bf16[768,2048]{1,0:T(8,128)(2,1)} async-done(((bf16[768,256]{1,0:T(8,128)(2,1)}), bf16[768,2048]{1,0:T(8,128)(2,1)}) %all-gather.2.cloned.1.call-update) | async-done | bytes 3145744 | tf_op jit(solution)/shard_map/all_gather | solution.py:32
  76.8 0.0 copy-start.2
  76.8 0.0 copy-start.4
  76.8 6.3 %fusion.2 = f32[4,192,1024]{2,1,0:T(8,128)S(1)} fusion(bf16[4,192,2048]{2,1,0:T(8,128)(2,1)} %bitcast.90, bf16[1,2048,1024]{2,1,0:T(8,128)(2,1)} %param.11), kind=kOutput, calls=%fused_computation.2 | convolution fusion | flops 3221225472 | bytes 10485760 | tf_op jit(solution)/shard_map/secw,ewf->secf/dot_general | solution.py:38
  83.1 0.0 copy-done.2
  83.1 0.0 copy-done.4
  83.1 0.0 copy-start.3
  83.1 3.8 %fusion.9 = bf16[4,1,192,1024]{3,2,0,1:T(8,128)(2,1)S(1)} fusion(f32[4,192,1024]{2,1,0:T(8,128)S(1)} %fusion.2, bf16[4,192,2048]{2,1,0:T(8,128)(2,1)S(1)} %bitcast.91, bf16[1,2048,1024]{2,1,0:T(8,128)(2,1)S(1)} %copy-done.2), kind=kOutput, calls=%fused_computation.8 | convolution fusion | flops 3225944064 | bytes 12058624 | tf_op jit(solution)/shard_map/secw,ewf->secf/dot_general | solution.py:35
  87.0 0.0 copy-done.3
  87.0 4.8 %fusion.13 = bf16[2048,768]{0,1:T(8,128)(2,1)} fusion(bf16[768,1024]{1,0:T(8,128)(2,1)S(1)} %bitcast.92, bf16[1,1024,2048]{2,1,0:T(8,128)(2,1)S(1)} %copy-done.3), kind=kOutput, calls=%fused_computation.14 | convolution fusion | flops 3222798336 | bytes 8912896 | tf_op jit(solution)/shard_map/secf,efd->dsec/dot_general | solution.py:40
  91.8 0.0 copy-start
  91.8 0.0 copy-start.1
  91.8 0.0 reduce-scatter.2.cloned.1.call-update
  91.8 38.8 %reduce-scatter.2.cloned.1.call-done = bf16[256,768]{0,1:T(8,128)(2,1)} async-done(((bf16[2048,768]{0,1:T(8,128)(2,1)}), bf16[256,768]{0,1:T(8,128)(2,1)}) %reduce-scatter.2.cloned.1.call-update) | async-done | bytes 393232 | tf_op jit(solution)/shard_map/reduce_scatter | solution.py:41
  130.6 3.6 %all-to-all-start.1 = ((bf16[256,4,192]{0,2,1:T(8,128)(2,1)}), bf16[256,4,192]{0,2,1:T(8,128)(2,1)S(1)}, u32[]{:S(2)}, u32[]{:S(2)}) async-start(bf16[256,4,192]{0,2,1:T(8,128)(2,1)} %bitcast.81), calls=%async_computation.2 | async-start | bytes 786432 | tf_op jit(solution)/shard_map/all_to_all | solution.py:49
  134.2 0.0 copy-done
  134.2 5.9 %all-to-all-done.1 = bf16[256,4,192]{0,2,1:T(8,128)(2,1)S(1)} async-done(((bf16[256,4,192]{0,2,1:T(8,128)(2,1)}), bf16[256,4,192]{0,2,1:T(8,128)(2,1)S(1)}, u32[]{:S(2)}, u32[]{:S(2)}) %all-to-all-start.1) | async-done | bytes 393248 | tf_op jit(solution)/shard_map/all_to_all | solution.py:49
  140.1 0.4 convolution_multiply_fusion.1
  140.5 0.4 multiply_reduce_fusion
  140.9 15.4 %psum.15 = f32[256]{0:T(256)S(1)} all-reduce(f32[256]{0:T(256)S(1)} %get-tuple-element.9), channel_id=1, replica_groups=mesh['ep'=4,'tp'=8] {'tp'}, use_global_device_ids=true, to_apply=%region_7.8 | all-reduce | flops 256 | bytes 2048 | tf_op jit(solution)/shard_map/psum | solution.py:56
  156.3 0.0 copy-done.1
  156.3 0.1 multiply_convert_fusion
  156.4 0.8 copy.23
  (6 shorter events, 0.1 us)
Async XLA Ops:
  6.5 70.3 %all-gather.2.cloned.1.call-start = ((), (), s32[]{:S(2)}) async-start(), calls=%async_computation.3 | async-start | bytes 3538944 | tf_op jit(solution)/shard_map/all_gather | solution.py:32
  40.8 89.8 %reduce-scatter.2.cloned.1.call-start = ((), (), s32[]{:S(2)}) async-start(), calls=%async_computation.4 | async-start | bytes 3538944 | tf_op jit(solution)/shard_map/reduce_scatter | solution.py:41
  76.8 6.3 %copy-start.2 = (bf16[1,2048,1024]{2,1,0:T(8,128)(2,1)S(1)}, bf16[1,2048,1024]{2,1,0:T(8,128)(2,1)}, u32[]{:S(2)}) copy-start(bf16[1,2048,1024]{2,1,0:T(8,128)(2,1)} %param.10) | copy-start | bytes 12582916
  76.8 6.3 %copy-start.4 = (bf16[768,2048]{1,0:T(8,128)(2,1)S(1)}, bf16[768,2048]{1,0:T(8,128)(2,1)}, u32[]{:S(2)}) copy-start(bf16[768,2048]{1,0:T(8,128)(2,1)} %all-gather.2.cloned.1.call-done) | copy-start | bytes 9437188
  83.1 3.9 %copy-start.3 = (bf16[1,1024,2048]{2,1,0:T(8,128)(2,1)S(1)}, bf16[1,1024,2048]{2,1,0:T(8,128)(2,1)}, u32[]{:S(2)}) copy-start(bf16[1,1024,2048]{2,1,0:T(8,128)(2,1)} %param.12) | copy-start | bytes 12582916
  91.8 42.4 %copy-start = (f32[256,2]{0,1:T(2,128)S(1)}, f32[256,2]{0,1:T(2,128)}, u32[]{:S(2)}) copy-start(f32[256,2]{0,1:T(2,128)} %param.14) | copy-start | bytes 6148
  91.8 64.5 %copy-start.1 = (f32[256]{0:T(256)S(1)}, f32[256]{0:T(256)}, u32[]{:S(2)}) copy-start(f32[256]{0:T(256)} %param.15) | copy-start | bytes 3076
  130.6 9.5 %all-to-all-start.1 = ((bf16[256,4,192]{0,2,1:T(8,128)(2,1)}), bf16[256,4,192]{0,2,1:T(8,128)(2,1)S(1)}, u32[]{:S(2)}, u32[]{:S(2)}) async-start(bf16[256,4,192]{0,2,1:T(8,128)(2,1)} %bitcast.81), calls=%async_computation.2 | async-start | bytes 786432 | tf_op jit(solution)/shard_map/all_to_all | solution.py:49
Sparse Core Ops, SparseCore 0:
  40.9 35.8 all-gather.1
  91.9 38.5 reduce-scatter.1
where the time goes:
time: 164 us
  waiting for transfers between devices  80.6 us (49%)
  blocking collectives  43.6 us (27%)
  matrix products  17 us (10%)
  between operations  13.5 us (8%)
  starting transfers between devices  3.69 us (2%)
  other arithmetic  3.35 us (2%)
  local copies, waits for them, and re-layouts  2.31 us (1%)
    reduce_scatter x1, waiting for transfers between devices, local(): lax.psum_scatter(product.reshape(lax.axis_size('tp') * part_width, groups...  38.8 us
    all_gather x1, waiting for transfers between devices, local(): fragment = lax.all_gather(arrived, 'tp', axis=1, tiled=True)  35.9 us
    psum x1, blocking collectives, local(): input_sq = lax.psum(jnp.sum(values * values, axis=-1), 'tp')  18.1 us
    psum x1, blocking collectives, local(): output_sq = lax.psum(jnp.sum(combined * combined, axis=-1), 'tp')  15.4 us
    all_to_all x1, blocking collectives, local(): lax.all_to_all(outgoing, 'ep', split_axis=0, concat_axis=0, tiled=True)  10.1 us
    dot_general x1, matrix products, local(): jnp.einsum('secw,ewf->secf', grouped, expert_up, preferred_element_type=j...  6.28 us
    all_to_all x1, waiting for transfers between devices, local(): lax.all_to_all(summed, 'ep', split_axis=1, concat_axis=1, tiled=True)  5.87 us
    dot_general x1, matrix products, local(): jnp.einsum('secf,efd->dsec', hidden, expert_down, preferred_element_type=...  4.83 us
  transfers between devices with their start and end apart: 3, of which 3 were waited for; matrix products, arithmetic and copies ran while one was open for 0% of the time, Pallas kernels for 0%

commit v1 on v0

--- a/solution.py
+++ b/solution.py
@@ -4,6 +4,28 @@
 from jax.sharding import PartitionSpec as P
 
 EPSILON = 1e-06
+
+
+def in_order(tiles, dim):
+    tiles = jnp.moveaxis(tiles, 0, dim)
+    dims = tiles.shape
+    return tiles.reshape(*dims[:dim], dims[dim] * dims[dim + 1], *dims[dim + 2 :])
+
+
+def grow_blocks(array, axis):
+    size = lax.axis_size(axis)
+    pieces = array[None]
+    for level in range(size.bit_length() - 1):
+        apart = 1 << level
+        partner_block = lax.ppermute(pieces, axis, [(i, i ^ apart) for i in range(size)])
+        both = jnp.stack([pieces, partner_block])
+        upper = lax.axis_index(axis) >> level & 1
+        pieces = jnp.where(upper == 0, both, both[::-1]).reshape(-1, *array.shape)
+    return pieces
+
+
+def gather_by_bits(x, axis, dim):
+    return in_order(grow_blocks(x, axis), dim)
 
 
 def local(tokens, pre_gain, expert_gate, expert_up, expert_down, routes, route_weights, post_gain):
@@ -29,7 +51,7 @@
     dispatch = first_pick + second_pick
     outgoing = jnp.dot(dispatch, normed, preferred_element_type=jnp.float32).astype(jnp.bfloat16)
     arrived = lax.all_to_all(outgoing, "ep", split_axis=0, concat_axis=0, tiled=True)
-    fragment = lax.all_gather(arrived, "tp", axis=1, tiled=True)
+    fragment = gather_by_bits(arrived, "tp", 1)
     count = fragment.shape[1]
     grouped = fragment.reshape(groups, local_experts, capacity, count)
     gate_pre = jnp.einsum(

time: 164 us -> 232 us (1.41)
  waiting for transfers between devices: 80.6 us -> 133 us
  local copies, waits for them, and re-layouts: 2.31 us -> 12 us
  other arithmetic: 3.35 us -> 9.15 us
    ppermute x0 -> x3, waiting for transfers between devices: none -> 90.3 us  [grow_blocks(): lax.ppermute(pieces, axis, [(i, i ^ apart) for i in range(size)])]
    all_gather x1 -> x0, waiting for transfers between devices: 35.9 us -> none  [local(): fragment = lax.all_gather(arrived, 'tp', axis=1, tiled=True)]
    another operation x0 -> x2, local copies, waits for them, and re-layouts: none -> 5.41 us
    reshape x0 -> x2, local copies, waits for them, and re-layouts: none -> 4.24 us  [grow_blocks(): pieces = jnp.where(upper == 0, both, both[::-1]).reshape(-1, *array.shape)]
    another operation x2 -> x6, other arithmetic: 1.41 us -> 5.25 us  [the longest x4 3.85 us: grow_blocks(): both = jnp.stack([pieces, partner_block])]
  transfers between devices with their start and end apart: 3 -> 5, of which waited for: 3 -> 5; matrix products, arithmetic and copies ran while one was open for 0% -> 1% of each run, Pallas kernels for 0% -> 0%
where the time goes in v1:
time: 232 us
  waiting for transfers between devices  133 us (57%)
  blocking collectives  43.4 us (19%)
  matrix products  16.2 us (7%)
  between operations  13.6 us (6%)
  local copies, waits for them, and re-layouts  12 us (5%)
  other arithmetic  9.15 us (4%)
  starting transfers between devices  3.78 us (2%)
    ppermute x3, waiting for transfers between devices, grow_blocks(): lax.ppermute(pieces, axis, [(i, i ^ apart) for i in range(size)])  90.3 us
    reduce_scatter x1, waiting for transfers between devices, local(): lax.psum_scatter(product.reshape(lax.axis_size('tp') * part_width, groups...  37.2 us
    psum x1, blocking collectives, local(): input_sq = lax.psum(jnp.sum(values * values, axis=-1), 'tp')  18.1 us
    psum x1, blocking collectives, local(): output_sq = lax.psum(jnp.sum(combined * combined, axis=-1), 'tp')  15.4 us
    all_to_all x1, blocking collectives, local(): lax.all_to_all(outgoing, 'ep', split_axis=0, concat_axis=0, tiled=True)  9.94 us
    all_to_all x1, waiting for transfers between devices, local(): lax.all_to_all(summed, 'ep', split_axis=1, concat_axis=1, tiled=True)  5.87 us
    dot_general x1, matrix products, local(): jnp.einsum('secw,ewf->secf', grouped, expert_up, preferred_element_type=j...  5.35 us
    dot_general x1, matrix products, local(): jnp.einsum('secf,efd->dsec', hidden, expert_down, preferred_element_type=...  5.01 us
  transfers between devices with their start and end apart: 5, of which 5 were waited for; matrix products, arithmetic and copies ran while one was open for 1% of the time, Pallas kernels for 0%

profile of v1, /device:TPU:0, one launch (start us, length us, event | category | flops | bytes accessed | tf_op | source)
XLA Modules:
  0.0 231.6 jit_solution(14586982678000928809)
XLA Ops:
  6.5 0.0 reduce-scatter.2.cloned.1.call-start
  6.5 0.8 copy.26
  7.4 0.1 eq.70
  7.5 0.1 eq.66
  7.7 1.2 reduce-window.6
  8.9 0.2 slice_reduce_fusion
  9.1 0.2 reduce-window.9
  9.3 0.1 add_bitcast_fusion
  9.4 0.1 reshape.65
  9.5 0.1 copy.28
  9.6 0.7 multiply_add_fusion
  10.3 1.0 fusion.30
  11.3 18.1 %psum.14 = f32[256]{0:T(256)S(1)} all-reduce(f32[256]{0:T(256)S(1)} %fusion.30), channel_id=1, replica_groups=mesh['ep'=4,'tp'=8] {'tp'}, use_global_device_ids=true, to_apply=%region_4.5 | all-reduce | flops 256 | bytes 2048 | tf_op jit(solution)/shard_map/psum | solution.py:39
  29.4 1.3 convolution_convert_fusion
  30.7 9.9 %all_to_all.21 = bf16[4,192,256]{2,1,0:T(8,128)(2,1)S(1)} all-to-all(bf16[4,192,256]{2,1,0:T(8,128)(2,1)S(1)} %bitcast.99), channel_id=1, replica_groups=mesh['ep'=4,'tp'=8] {'ep'}, dimensions={0} | all-to-all | bytes 786432 | tf_op jit(solution)/shard_map/all_to_all | solution.py:53
  40.7 0.0 collective-permute-start
  40.7 1.7 collective-permute-done
  42.4 0.1 pad_maximum_fusion.2
  42.5 0.2 fusion.22
  42.7 0.1 collective-permute-start.1
  42.8 19.6 %collective-permute-done.1 = bf16[2,768,256]{2,1,0:T(8,128)(2,1)S(1)} collective-permute-done((bf16[2,768,256]{2,1,0:T(8,128)(2,1)S(1)}, bf16[2,768,256]{2,1,0:T(8,128)(2,1)S(1)}, u32[]{:S(2)}, u32[]{:S(2)}) %collective-permute-start.1) | collective-permute-done | bytes 786464 | tf_op jit(solution)/shard_map/ppermute | solution.py:20
  62.3 0.1 pad_maximum_fusion.1
  62.5 0.3 reverse_select_fusion.1
  62.8 1.2 copy.29
  64.0 0.1 collective-permute-start.2
  64.1 1.2 copy.30
  65.3 69.0 %collective-permute-done.2 = bf16[4,768,256]{2,0,1:T(4,128)(2,1)} collective-permute-done((bf16[4,768,256]{2,0,1:T(4,128)(2,1)S(1)}, bf16[4,768,256]{2,0,1:T(4,128)(2,1)}, u32[]{:S(2)}, u32[]{:S(2)}) %collective-permute-start.2) | collective-permute-done | bytes 1572896 | tf_op jit(solution)/shard_map/ppermute | solution.py:20
  134.4 3.4 %pad_maximum_fusion = bf16[2,4,768,256]{3,1,0,2:T(4,128)(2,1)S(1)} fusion(bf16[1,4,768,256]{3,1,0,2:T(4,128)(2,1)} %bitcast.13, bf16[1,4,768,256]{3,1,0,2:T(4,128)(2,1)S(1)} %copy.30), kind=kLoop, calls=%fused_computation.8 | loop fusion | flops 1572864 | bytes 6291456 | tf_op jit(solution)/shard_map/stack | solution.py:21
  137.8 1.6 reverse_select_fusion
  139.4 3.0 %reshape.68 = bf16[8,768,256]{2,0,1:T(8,128)(2,1)} reshape(bf16[2,4,768,256]{3,1,0,2:T(4,128)(2,1)S(1)} %reverse_select_fusion) | data formatting | bytes 6291456 | tf_op jit(solution)/shard_map/reshape | solution.py:23
  142.5 4.2 %reshape.69 = bf16[4,192,2048]{2,1,0:T(8,128)(2,1)S(1)} reshape(bf16[768,8,256]{2,1,0:T(8,128)(2,1)} %bitcast.92) | data formatting | bytes 6291456 | tf_op jit(solution)/shard_map/reshape.4
  146.7 0.0 copy-start.2
  146.7 5.3 %fusion.2 = f32[4,192,1024]{2,1,0:T(8,128)S(1)} fusion(bf16[4,192,2048]{2,1,0:T(8,128)(2,1)S(1)} %reshape.69, bf16[1,2048,1024]{2,1,0:T(8,128)(2,1)} %param.11), kind=kOutput, calls=%fused_computation.3 | convolution fusion | flops 3221225472 | bytes 10485760 | tf_op jit(solution)/shard_map/secw,ewf->secf/dot_general | solution.py:60
  152.0 0.0 copy-done.2
  152.1 0.0 copy-start.3
  152.1 3.8 %fusion.9 = bf16[4,1,192,1024]{3,2,0,1:T(8,128)(2,1)S(1)} fusion(f32[4,192,1024]{2,1,0:T(8,128)S(1)} %fusion.2, bf16[4,192,2048]{2,1,0:T(8,128)(2,1)S(1)} %reshape.69, bf16[1,2048,1024]{2,1,0:T(8,128)(2,1)S(1)} %copy-done.2), kind=kOutput, calls=%fused_computation.10 | convolution fusion | flops 3225944064 | bytes 12058624 | tf_op jit(solution)/shard_map/secw,ewf->secf/dot_general | solution.py:57
  155.9 0.0 copy-done.3
  155.9 5.0 %fusion.13 = bf16[2048,768]{0,1:T(8,128)(2,1)} fusion(bf16[768,1024]{1,0:T(8,128)(2,1)S(1)} %bitcast.108, bf16[1,1024,2048]{2,1,0:T(8,128)(2,1)S(1)} %copy-done.3), kind=kOutput, calls=%fused_computation.16 | convolution fusion | flops 3222798336 | bytes 8912896 | tf_op jit(solution)/shard_map/secf,efd->dsec/dot_general | solution.py:62
  160.9 0.0 copy-start
  160.9 0.0 copy-start.1
  160.9 0.0 reduce-scatter.2.cloned.1.call-update
  161.0 37.2 %reduce-scatter.2.cloned.1.call-done = bf16[256,768]{0,1:T(8,128)(2,1)} async-done(((bf16[2048,768]{0,1:T(8,128)(2,1)}), bf16[256,768]{0,1:T(8,128)(2,1)}) %reduce-scatter.2.cloned.1.call-update) | async-done | bytes 393232 | tf_op jit(solution)/shard_map/reduce_scatter | solution.py:63
  198.2 3.6 %all-to-all-start.1 = ((bf16[256,4,192]{0,2,1:T(8,128)(2,1)}), bf16[256,4,192]{0,2,1:T(8,128)(2,1)S(1)}, u32[]{:S(2)}, u32[]{:S(2)}) async-start(bf16[256,4,192]{0,2,1:T(8,128)(2,1)} %bitcast.98), calls=%async_computation.2 | async-start | bytes 786432 | tf_op jit(solution)/shard_map/all_to_all | solution.py:71
  201.8 0.0 copy-done
  201.8 5.9 %all-to-all-done.1 = bf16[256,4,192]{0,2,1:T(8,128)(2,1)S(1)} async-done(((bf16[256,4,192]{0,2,1:T(8,128)(2,1)}), bf16[256,4,192]{0,2,1:T(8,128)(2,1)S(1)}, u32[]{:S(2)}, u32[]{:S(2)}) %all-to-all-start.1) | async-done | bytes 393248 | tf_op jit(solution)/shard_map/all_to_all | solution.py:71
  207.7 0.4 convolution_multiply_fusion.1
  208.1 0.4 multiply_reduce_fusion
  208.4 15.4 %psum.15 = f32[256]{0:T(256)S(1)} all-reduce(f32[256]{0:T(256)S(1)} %get-tuple-element.11), channel_id=1, replica_groups=mesh['ep'=4,'tp'=8] {'tp'}, use_global_device_ids=true, to_apply=%region_7.8 | all-reduce | flops 256 | bytes 2048 | tf_op jit(solution)/shard_map/psum | solution.py:78
  223.9 0.0 copy-done.1
  223.9 0.1 multiply_convert_fusion
  224.0 0.8 copy.31
  (6 shorter events, 0.1 us)
Async XLA Ops:
  6.5 191.6 %reduce-scatter.2.cloned.1.call-start = ((), (), s32[]{:S(2)}) async-start(), calls=%async_computation.3 | async-start | bytes 3538944 | tf_op jit(solution)/shard_map/reduce_scatter | solution.py:63
  40.7 1.7 collective-permute-start
  42.7 19.6 %collective-permute-start.1 = (bf16[2,768,256]{2,1,0:T(8,128)(2,1)S(1)}, bf16[2,768,256]{2,1,0:T(8,128)(2,1)S(1)}, u32[]{:S(2)}, u32[]{:S(2)}) collective-permute-start(bf16[2,768,256]{2,1,0:T(8,128)(2,1)S(1)} %get-tuple-element.6), channel_id=1, source_target_pairs={{0,2},{1,3},{2,0},{3,1},{4,6},{5,7},{6,4},{7,5},{8,10},{9,11},{10,... | collective-permute-start | bytes 2359304 | tf_op jit(solution)/shard_map/ppermute | solution.py:20
  64.0 70.4 %collective-permute-start.2 = (bf16[4,768,256]{2,0,1:T(4,128)(2,1)S(1)}, bf16[4,768,256]{2,0,1:T(4,128)(2,1)}, u32[]{:S(2)}, u32[]{:S(2)}) collective-permute-start(bf16[4,768,256]{2,0,1:T(4,128)(2,1)S(1)} %copy.29), channel_id=1, source_target_pairs={{0,4},{1,5},{2,6},{3,7},{4,0},{5,1},{6,2},{7,3},{8,12},{9,13},{10,... | collective-permute-start | bytes 4718600 | tf_op jit(solution)/shard_map/ppermute | solution.py:20
  146.7 5.4 %copy-start.2 = (bf16[1,2048,1024]{2,1,0:T(8,128)(2,1)S(1)}, bf16[1,2048,1024]{2,1,0:T(8,128)(2,1)}, u32[]{:S(2)}) copy-start(bf16[1,2048,1024]{2,1,0:T(8,128)(2,1)} %param.10) | copy-start | bytes 12582916
  152.1 3.9 %copy-start.3 = (bf16[1,1024,2048]{2,1,0:T(8,128)(2,1)S(1)}, bf16[1,1024,2048]{2,1,0:T(8,128)(2,1)}, u32[]{:S(2)}) copy-start(bf16[1,1024,2048]{2,1,0:T(8,128)(2,1)} %param.12) | copy-start | bytes 12582916
  160.9 40.9 %copy-start = (f32[256,2]{0,1:T(2,128)S(1)}, f32[256,2]{0,1:T(2,128)}, u32[]{:S(2)}) copy-start(f32[256,2]{0,1:T(2,128)} %param.14) | copy-start | bytes 6148
  160.9 62.9 %copy-start.1 = (f32[256]{0:T(256)S(1)}, f32[256]{0:T(256)}, u32[]{:S(2)}) copy-start(f32[256]{0:T(256)} %param.15) | copy-start | bytes 3076
  198.2 9.5 %all-to-all-start.1 = ((bf16[256,4,192]{0,2,1:T(8,128)(2,1)}), bf16[256,4,192]{0,2,1:T(8,128)(2,1)S(1)}, u32[]{:S(2)}, u32[]{:S(2)}) async-start(bf16[256,4,192]{0,2,1:T(8,128)(2,1)} %bitcast.98), calls=%async_computation.2 | async-start | bytes 786432 | tf_op jit(solution)/shard_map/all_to_all | solution.py:71
Sparse Core Ops, SparseCore 0:
  161.1 37.0 reduce-scatter.1
